TPU v7x, 512 devices: a whole 4x4x16 slice. The times are simulated.
512 devices in a mesh: sp: 16 (over z), fs: 4 (over y), tp: 8 (over x, core).
Axes of the slice: x: 4, y: 4, z: 16, core: 2. Of those that a mesh axis runs over, the one named last changes fastest.
Arguments:
- tokens: bfloat16 [4, 4096, 2048], P('fs', ('sp', 'tp')), may hold values from -6 to 6
- query_weight: bfloat16 [2048, 2048], P(('sp', 'fs'), 'tp'), may hold values from -0.125 to 0.125
- forget_weight: bfloat16 [2048, 2048], P(('sp', 'fs'), 'tp'), may hold values from -0.125 to 0.125
- value_weight: bfloat16 [2048, 2048], P(('sp', 'fs'), 'tp'), may hold values from -0.125 to 0.125
- convolution_gate_weight: bfloat16 [2048, 1024], P(('sp', 'fs'), 'tp'), may hold values from -0.125 to 0.125
- convolution_multiplier_weight: bfloat16 [2048, 1024], P(('sp', 'fs'), 'tp'), may hold values from -0.125 to 0.125
- convolution_input_weight: bfloat16 [2048, 1024], P(('sp', 'fs'), 'tp'), may hold values from -0.125 to 0.125
- gate_headroom: float32 [2048], P('tp'), may hold values from 2.4414063e-05 to 0.06
- added_log_rate: float32 [4, 16, 4096], P('fs', 'tp', 'sp'), may hold values from -1.6 to 0
- initial_state: float32 [4, 16, 128, 128], P('fs', 'tp'), may hold values from -0.25 to 0.25
- head_norm_gain: float32 [2048], P('tp'), may hold values from 0.1 to 1.9
- convolution_taps: float32 [3, 1024], P(None, 'tp'), may hold values from -3.5 to 3.5
- convolution_bias: float32 [1024], P('tp'), may hold values from -4 to 4
- recurrence_output_weight: bfloat16 [2048, 2048], P('tp', ('sp', 'fs')), may hold values from -0.109375 to 0.109375
- convolution_output_weight: bfloat16 [1024, 2048], P('tp', ('sp', 'fs')), may hold values from -0.109375 to 0.109375
Outputs:
- mixed: bfloat16 [4, 4096, 2048], P('fs', ('sp', 'tp'))
All inputs are finite; a program needn't handle non-finite values.
Results may differ from a plain program's by a relative error of at most 0.018.
Values may be sent and summed in bfloat16 or wider, within the bound.
A program may use at most 64 MiB of HBM per device.

v0:
```python
import jax
import jax.numpy as jnp
from jax import lax
from jax.sharding import PartitionSpec as P

DK = 128
KW = 3
BLOCK_POSITIONS = 64


def gather_turned(arrays, axis, dims):
    turned = [jnp.moveaxis(a, dim, 0) for a, dim in zip(arrays, dims)]
    widths = [t[0].size for t in turned]
    both = jnp.concatenate([t.reshape(-1, w) for t, w in zip(turned, widths)], axis=1)
    result = lax.all_gather(both, axis, axis=0, tiled=True)
    parts = jnp.split(result, [sum(widths[:k]) for k in range(1, len(widths))], axis=1)
    return tuple(
        (
            jnp.moveaxis(b.reshape(-1, *t.shape[1:]), 0, dim)
            for b, t, dim in zip(parts, turned, dims)
        )
    )


def copy_for_each(value, axis):
    copies = jnp.broadcast_to(value, (lax.axis_size(axis), *value.shape))
    return lax.all_to_all(copies, axis, split_axis=0, concat_axis=0, tiled=True)


def in_order(parts, dim):
    parts = jnp.moveaxis(parts, 0, dim)
    dims = parts.shape
    return parts.reshape(*dims[:dim], dims[dim] * dims[dim + 1], *dims[dim + 2 :])


def gather_directly(value, axis, dim):
    parts = copy_for_each(value, axis)
    return in_order(parts, dim)


def carried_in(part, axis, combine, identity):
    place = lax.axis_index(axis)
    gathered = jax.tree.map(lambda a: lax.all_gather(a, axis), part)
    state = jax.tree.map(lambda a, e: jnp.zeros_like(a) + jnp.asarray(e, a.dtype), part, identity)

    def one(hop, state):
        return combine(
            state, jax.tree.map(lambda a: lax.dynamic_index_in_dim(a, hop, 0, False), gathered)
        )

    return lax.fori_loop(0, place, one, state)


def from_behind(block, axis, distance):
    devices = range(lax.axis_size(axis))
    route = [(i - distance, i) for i in devices if i - distance in devices]
    return lax.ppermute(block, axis, route)


def in_blocks(value, dim, peers):
    before, after = (value.shape[:dim], value.shape[dim + 1 :])
    return jnp.moveaxis(value.reshape(*before, peers, -1, *after), dim, 0)


def summed_on_arrival(value, axis, dim):
    parts = in_blocks(value, dim, lax.axis_size(axis))
    arrived = lax.all_to_all(parts, axis, split_axis=0, concat_axis=0, tiled=True)
    return arrived.astype(jnp.float32).sum(axis=0)


def to_blocks(values, number_of_heads):
    number_of_blocks = values.shape[0] // BLOCK_POSITIONS
    return jnp.transpose(
        values.reshape(number_of_blocks, BLOCK_POSITIONS, number_of_heads, DK), (2, 0, 1, 3)
    )


def within_block_recurrence(
    query_vectors, forget_logits, value_vectors, gate_headroom, extra_rates
):
    number_of_heads = extra_rates.shape[0]
    number_of_blocks = query_vectors.shape[0] // BLOCK_POSITIONS
    query_scaled = to_blocks(query_vectors.astype(jnp.float32), number_of_heads) * DK ** (-0.5)
    gated_key = to_blocks(
        gate_headroom[None, :] * jax.nn.sigmoid(-forget_logits.astype(jnp.float32)), number_of_heads
    )
    forget_log_rate = (
        jnp.log1p(-gated_key)
        + extra_rates.reshape(number_of_heads, number_of_blocks, BLOCK_POSITIONS)[..., None]
    )
    values = to_blocks(value_vectors.astype(jnp.float32), number_of_heads)
    cumulative = jnp.cumsum(forget_log_rate, axis=2)
    query_decayed = query_scaled * jnp.exp(cumulative)
    key_decayed = gated_key * jnp.exp(-cumulative)
    scores = jnp.einsum("hnik,hnjk->hnij", query_decayed, key_decayed)
    causal = jnp.tril(jnp.ones((BLOCK_POSITIONS, BLOCK_POSITIONS), dtype=bool))
    scores = jnp.where(causal, scores, 0.0)
    within = jnp.einsum("hnij,hnjv->hniv", scores, values)
    final_log = cumulative[:, :, -1, :]
    contrib = jnp.einsum(
        "hnck,hncv->hnkv", gated_key * jnp.exp(final_log[:, :, None, :] - cumulative), values
    )
    decays = jnp.exp(final_log)

    def advance(current, block_pair):
        return (block_pair[0][..., None] * current + block_pair[1], current)

    empty_state = jnp.zeros((number_of_heads, DK, DK), jnp.float32)
    local_total, entering = lax.scan(
        advance, empty_state, (jnp.moveaxis(decays, 1, 0), jnp.moveaxis(contrib, 1, 0))
    )
    entering = jnp.moveaxis(entering, 0, 1)
    before = jnp.exp(jnp.cumsum(final_log, axis=1) - final_log)
    device_decay = jnp.exp(jnp.sum(final_log, axis=1))
    return (query_decayed, within, entering, before, device_decay, local_total)


def finish(query_decayed, within, entering, before, carried, head_norm_gain):
    number_of_heads = query_decayed.shape[0]
    states = entering + before[..., None] * carried[:, None]
    carried_term = jnp.einsum("hnck,hnkv->hncv", query_decayed, states)
    length = query_decayed.shape[1] * BLOCK_POSITIONS
    recurrence_unnormed = jnp.transpose(within + carried_term, (1, 2, 0, 3)).reshape(
        length, number_of_heads, DK
    )
    mean_square = jnp.mean(recurrence_unnormed * recurrence_unnormed, axis=-1, keepdims=True)
    rec_out = (
        recurrence_unnormed
        * lax.rsqrt(mean_square + 1e-06)
        * head_norm_gain.reshape(number_of_heads, DK)
    )
    return rec_out.reshape(length, number_of_heads * DK).astype(jnp.bfloat16)


def chain_combine(earlier_part, later_part):
    return (
        earlier_part[0] * later_part[0],
        later_part[0][..., None] * earlier_part[1] + later_part[1],
    )


def shards(
    tokens,
    query_weight,
    forget_weight,
    value_weight,
    convolution_gate_weight,
    convolution_multiplier_weight,
    convolution_input_weight,
    gate_headroom,
    added_log_rate,
    initial_state,
    head_norm_gain,
    convolution_taps,
    convolution_bias,
    recurrence_output_weight,
    convolution_output_weight,
):
    own_rows = tokens[0]
    gathered = gather_turned(
        (
            query_weight,
            forget_weight,
            value_weight,
            convolution_gate_weight,
            convolution_multiplier_weight,
            convolution_input_weight,
            recurrence_output_weight,
            convolution_output_weight,
        ),
        ("sp", "fs"),
        (0, 0, 0, 0, 0, 0, 1, 1),
    )
    in_weights = gathered[:6]
    out_rec = gathered[6]
    out_conv = gathered[7]
    block_rows = gather_directly(own_rows, "tp", 0)
    projected = jnp.concatenate(
        [
            jnp.dot(block_rows, weight, preferred_element_type=jnp.float32).astype(jnp.bfloat16)
            for weight in in_weights
        ],
        axis=1,
    )
    rec_width = query_weight.shape[1]
    conv_width = convolution_gate_weight.shape[1]
    query_vectors = projected[:, :rec_width]
    forget_logits = projected[:, rec_width : 2 * rec_width]
    value_vectors = projected[:, 2 * rec_width : 3 * rec_width]
    conv_base = 3 * rec_width
    conv_gate = projected[:, conv_base : conv_base + conv_width]
    conv_mult = projected[:, conv_base + conv_width : conv_base + 2 * conv_width]
    conv_input = projected[:, conv_base + 2 * conv_width : conv_base + 3 * conv_width]
    query_decayed, within, entering, before, device_decay, local_total = within_block_recurrence(
        query_vectors, forget_logits, value_vectors, gate_headroom, added_log_rate[0]
    )
    conv_prod = conv_mult.astype(jnp.float32) * conv_input.astype(jnp.float32)
    length = conv_prod.shape[0]
    tail_rows = conv_prod[length - (KW - 1) :]
    unit_decay = jnp.ones_like(device_decay)
    empty_state = jnp.zeros_like(local_total)
    prior_decay, prior_state = carried_in(
        (device_decay, local_total), "sp", chain_combine, (unit_decay, empty_state)
    )
    prior_rows = from_behind(tail_rows, "sp", 1)
    carried = prior_decay[..., None] * initial_state[0] + prior_state
    rec_out = finish(query_decayed, within, entering, before, carried, head_norm_gain)
    extended = jnp.concatenate([prior_rows, conv_prod], axis=0)
    conv_y = jnp.broadcast_to(convolution_bias[None, :], conv_prod.shape)
    for j in range(KW):
        conv_y = conv_y + convolution_taps[j][None, :] * extended[j : j + length]
    conv_out = (conv_gate.astype(jnp.float32) * conv_y).astype(jnp.bfloat16)
    mixed = summed_on_arrival(
        (
            jnp.dot(rec_out, out_rec, preferred_element_type=jnp.float32)
            + jnp.dot(conv_out, out_conv, preferred_element_type=jnp.float32)
        ).astype(jnp.bfloat16),
        "tp",
        0,
    )
    return mixed.astype(jnp.bfloat16)[None]


def solution(mesh):
    in_specs = (
        P("fs", ("sp", "tp"), None),
        P(("sp", "fs"), "tp"),
        P(("sp", "fs"), "tp"),
        P(("sp", "fs"), "tp"),
        P(("sp", "fs"), "tp"),
        P(("sp", "fs"), "tp"),
        P(("sp", "fs"), "tp"),
        P("tp"),
        P("fs", "tp", "sp"),
        P("fs", "tp", None, None),
        P("tp"),
        P(None, "tp"),
        P("tp"),
        P("tp", ("sp", "fs")),
        P("tp", ("sp", "fs")),
    )
    out_specs = P("fs", ("sp", "tp"), None)
    return jax.shard_map(shards, mesh=mesh, in_specs=in_specs, out_specs=out_specs, check_vma=False)
```

profile of v0, /device:TPU:496, one launch (start us, length us, event | category | flops | bytes accessed | tf_op | source)
XLA Modules:
  0.0 286.7 jit_solution(150869934221793700)
XLA Ops:
  6.5 0.7 constant_dynamic-update-slice_fusion.7
  7.3 0.7 constant_dynamic-update-slice_fusion.6
  8.0 0.7 constant_dynamic-update-slice_fusion.5
  8.7 0.7 constant_dynamic-update-slice_fusion.4
  9.4 0.7 constant_dynamic-update-slice_fusion.3
  10.1 0.7 constant_dynamic-update-slice_fusion.2
  10.8 0.7 constant_dynamic-update-slice_fusion.1
  11.5 0.7 constant_dynamic-update-slice_fusion
  12.2 0.6 copy-done.1
  12.9 2.0 broadcast_in_dim.41
  14.9 4.3 %all-to-all-start = ((bf16[8,32,2048]{2,1,0:T(8,128)(2,1)}), bf16[8,32,2048]{2,1,0:T(8,128)(2,1)S(1)}, u32[]{:S(2)}, u32[]{:S(2)}) async-start(bf16[8,32,2048]{2,1,0:T(8,128)(2,1)} %broadcast_in_dim.41), calls=%async_computation | async-start | bytes 2097152 | tf_op jit(solution)/shard_map/all_to_all | solution.py:27
  19.2 0.0 all-gather.8.cloned.1.call-start
  19.3 0.8 add.73
  20.0 15.1 %all-to-all-done = bf16[8,32,2048]{2,1,0:T(8,128)(2,1)S(1)} async-done(((bf16[8,32,2048]{2,1,0:T(8,128)(2,1)}), bf16[8,32,2048]{2,1,0:T(8,128)(2,1)S(1)}, u32[]{:S(2)}, u32[]{:S(2)}) %all-to-all-start) | async-done | bytes 1048608 | tf_op jit(solution)/shard_map/all_to_all | solution.py:27
  35.2 124.9 %all-gather.6.cloned.1.call-done = bf16[2048,1536]{1,0:T(8,128)(2,1)} async-done(((bf16[32,1536]{1,0:T(8,128)(2,1)}), bf16[2048,1536]{1,0:T(8,128)(2,1)}) %all-gather.6.cloned.1.call-update) | async-done | bytes 6291472 | tf_op jit(solution)/shard_map/all_gather | solution.py:15
  160.0 1.7 fusion.8
  161.8 0.2 reshape.82
  162.0 0.2 copy.38
  162.2 0.1 fusion.32
  162.3 0.2 reduce_window_sum.22
  162.6 1.7 fusion.12
  164.3 0.1 copy.39
  164.5 0.3 convolution_bitcast_fusion
  164.8 0.7 while.26
  164.9 0.1 bitcast_add_fusion.8
  165.0 0.1 bitcast_add_fusion.8
  165.2 0.1 bitcast_add_fusion.8
  165.4 0.1 bitcast_add_fusion.8
  165.6 0.6 copy-done
  166.3 1.7 fusion.11
  168.0 0.2 reshape.81
  168.3 0.2 copy.36
  168.4 1.5 fusion.16
  170.0 1.5 fusion.15
  171.5 0.1 slice.29
  171.6 1.3 collective-permute-start
  172.9 27.9 %all-gather.2 = f32[16,2,128]{2,1,0:T(2,128)S(1)} all-gather(f32[1,2,128]{2,1,0:T(2,128)S(1)} %exponential_bitcast_fusion.1), channel_id=2, replica_groups=mesh['sp'=16,'fs'=4,'tp'=8] {'sp'}, dimensions={0}, use_global_device_ids=true | all-gather | bytes 17408 | tf_op jit(solution)/shard_map/all_gather | solution.py:43
  200.8 0.3 fusion.2
  201.1 34.5 %all-gather.8.cloned.1.call-done = f32[32,128,128]{2,1,0:T(8,128)} async-done(((f32[2,128,128]{2,1,0:T(8,128)}), f32[32,128,128]{2,1,0:T(8,128)}) %all-gather.8.cloned.1.call-update) | async-done | bytes 2097168 | tf_op jit(solution)/shard_map/all_gather | solution.py:43
  235.7 16.2 %while.25 = (s32[]{:T(128)}, f32[2,128]{1,0:T(2,128)S(1)}, f32[2,128,128]{2,1,0:T(8,128)S(1)}, s32[]{:T(128)}, f32[16,2,128]{2,1,0:T(2,128)S(1)}, /*index=5*/f32...) while((s32[]{:T(128)}, f32[2,128]{1,0:T(2,128)S(1)}, f32[2,128,128]{2,1,0:T(8,128)S(1)}, s32[]{:T(128)}, ...), condition=%wide.region_6.7_spmd, body=%wide.region_5.6_spmd.sunk | while | flops 65797 | bytes 398471 | solution.py:51
  235.7 1.0 bitcast_add_fusion.7
  236.8 1.0 bitcast_add_fusion.7
  237.9 1.0 bitcast_add_fusion.7
  239.0 1.0 bitcast_add_fusion.7
  240.0 1.0 bitcast_add_fusion.7
  241.1 1.0 bitcast_add_fusion.7
  242.2 1.0 bitcast_add_fusion.7
  243.3 1.0 bitcast_add_fusion.7
  244.3 1.0 bitcast_add_fusion.7
  245.4 1.0 bitcast_add_fusion.7
  246.5 1.0 bitcast_add_fusion.7
  247.6 1.0 bitcast_add_fusion.7
  248.6 1.0 bitcast_add_fusion.7
  249.7 1.0 bitcast_add_fusion.7
  250.8 1.0 bitcast_add_fusion.7
  251.8 0.1 fusion.48
  252.0 0.4 multiply_reduce_fusion
  252.4 0.1 copy.52
  252.5 0.2 copy.46
  252.8 0.3 mul.153
  253.1 1.7 fusion.19
  254.8 3.7 %fusion = bf16[256,2048]{1,0:T(8,128)(2,1)} fusion(f32[256,2048]{1,0:T(8,128)S(1)} %fusion.19, bf16[2048,1536]{1,0:T(8,128)(2,1)} %all-gather.6.cloned.1.call-done, f32[2,128]{0,1:T(8,128)S(1)} %collective-permute-done, f32[256,128]{0,1:T(8,128)S(1)} %fusion.15, bf16[256,2048]{1,0:T(8,128)(2,1)S(1)} %bitcast.116, f32[128]{0:T(128)S(1)} %get-tuple-element.133, ...), kind=kOutput, calls=%fused_computation.6 | convolution fusion | flops 269877248 | bytes 5377024 | tf_op jit(solution)/shard_map/dot_general | solution.py:216
  258.5 20.6 %all_to_all.10 = bf16[8,32,2048]{2,1,0:T(8,128)(2,1)S(1)} all-to-all(bf16[8,32,2048]{2,1,0:T(8,128)(2,1)} %bitcast.117), channel_id=1, replica_groups=mesh['sp'=16,'fs'=4,'tp'=8] {'tp'}, dimensions={0} | all-to-all | bytes 2097152 | tf_op jit(solution)/shard_map/all_to_all | solution.py:67
  279.0 0.8 reduce_sum.32
  (48 shorter events, 0.5 us)
Async XLA Ops:
  6.5 153.5 %all-gather.6.cloned.1.call-start = ((), (), s32[]{:S(2)}) async-start(), calls=%async_computation.2 | async-start | bytes 6389760 | tf_op jit(solution)/shard_map/all_gather | solution.py:15
  12.2 0.6 copy-start.1
  14.9 20.2 %all-to-all-start = ((bf16[8,32,2048]{2,1,0:T(8,128)(2,1)}), bf16[8,32,2048]{2,1,0:T(8,128)(2,1)S(1)}, u32[]{:S(2)}, u32[]{:S(2)}) async-start(bf16[8,32,2048]{2,1,0:T(8,128)(2,1)} %broadcast_in_dim.41), calls=%async_computation | async-start | bytes 2097152 | tf_op jit(solution)/shard_map/all_to_all | solution.py:27
  19.2 216.4 %all-gather.8.cloned.1.call-start = ((), (), s32[]{:S(2)}) async-start(), calls=%async_computation.3 | async-start | bytes 2228224 | tf_op jit(solution)/shard_map/all_gather | solution.py:43
  160.0 6.3 %copy-start.3 = (f32[3,128]{1,0:T(4,128)S(1)}, f32[3,128]{1,0:T(4,128)}, u32[]{:S(2)}) copy-start(f32[3,128]{1,0:T(4,128)} %param.30) | copy-start | bytes 4612
  165.6 0.7 copy-start
  165.6 86.3 %copy-start.2 = (f32[1,2,128,128]{3,2,1,0:T(8,128)S(1)}, f32[1,2,128,128]{3,2,1,0:T(8,128)}, u32[]{:S(2)}) copy-start(f32[1,2,128,128]{3,2,1,0:T(8,128)} %param.28) | copy-start | bytes 393220
  168.0 85.1 %copy-start.4 = (f32[256]{0:T(256)S(1)}, f32[256]{0:T(256)}, u32[]{:S(2)}) copy-start(f32[256]{0:T(256)} %param.29) | copy-start | bytes 3076
  171.6 83.2 %collective-permute-start = (f32[2,128]{0,1:T(8,128)S(1)}, f32[2,128]{0,1:T(8,128)S(1)}, u32[]{:S(2)}, u32[]{:S(2)}) collective-permute-start(f32[2,128]{0,1:T(8,128)S(1)} %slice.29), channel_id=1, source_target_pairs={{0,32},{32,64},{64,96},{96,128},{128,160},{160,192},{192,224},{224... | collective-permute-start | bytes 3080 | tf_op jit(solution)/shard_map/ppermute | solution.py:57
Sparse Core Ops, SparseCore 0:
  13.0 146.9 all-gather.5
  166.4 69.2 all-gather.7
where the time goes:
time: 288 us; the launch traced here: 287 us
  waiting for transfers between devices  175 us (61%)
  blocking collectives  48.4 us (17%)
  other arithmetic  17.6 us (6%)
  matrix products  14.6 us (5%)
  between operations  13.7 us (5%)
  local copies, waits for them, and re-layouts  11.5 us (4%)
  starting transfers between devices  5.63 us (2%)
    all_gather x1, waiting for transfers between devices, gather_turned(): result = lax.all_gather(both, axis, axis=0, tiled=True)  125 us
    all_gather x1, waiting for transfers between devices, carried_in(): gathered = jax.tree.map(lambda a: lax.all_gather(a, axis), part)  34.5 us
    all_gather x1, blocking collectives, carried_in(): gathered = jax.tree.map(lambda a: lax.all_gather(a, axis), part)  27.9 us
    all_to_all x1, blocking collectives, summed_on_arrival(): lax.all_to_all(parts, axis, split_axis=0, concat_axis=0, tiled=True)  20.6 us
    add x15, other arithmetic, chain_combine(): later_part[0][..., None] * earlier_part[1] + later_part[1]  15.4 us
    all_to_all x1, waiting for transfers between devices, copy_for_each(): return lax.all_to_all(copies, axis, split_axis=0, concat_axis=0, tiled=True)  15.1 us
    dot_general x5, matrix products, shards(): jnp.dot(block_rows, weight, preferred_element_type=jnp.float32)  8.21 us
    unnamed x18, local copies, waits for them, and re-layouts  6.28 us
  transfers between devices with their start and end apart: 4, of which 3 were waited for; matrix products, arithmetic and copies ran while one was open for 9% of the time, Pallas kernels for 0%

commit v1 on v0

v1 whole, which is shorter than its diff:
```python
import functools

import jax
import jax.numpy as jnp
from jax import lax
from jax.experimental import pallas as pl
from jax.experimental.pallas import tpu as pltpu
from jax.sharding import PartitionSpec as P

F32 = jnp.float32
BF16 = jnp.bfloat16
MESH = pl.DeviceIdType.MESH
DK = 128
BLOCK = 64
NX = 4
NY = 4


def dot(a, b):
    return lax.dot_general(a, b, (((1,), (0,)), ((), ())), preferred_element_type=F32)


def dot_nt(a, b):
    return lax.dot_general(a, b, (((1,), (1,)), ((), ())), preferred_element_type=F32)


def dot_tn(a, b):
    return lax.dot_general(a, b, (((0,), (0,)), ((), ())), preferred_element_type=F32)


def three_words(a):
    high = a.astype(BF16)
    rest = a - high.astype(F32)
    middle = rest.astype(BF16)
    low = (rest - middle.astype(F32)).astype(BF16)
    return high, middle, low


def layer(
    nz,
    tok,
    wq,
    wf,
    wv,
    wg,
    wm,
    wi,
    small,
    s0,
    wot,
    out,
    wbuf,
    wob,
    xbuf,
    sta,
    stb,
    spbuf,
    s0buf,
    sbuf,
    vbuf,
    kgbuf,
    cumbuf,
    offbuf,
    qbuf,
    recbuf,
    qbbuf,
    gatebuf,
    ext,
    halo,
    actr,
    actc,
    abuf,
    pbuf,
    rbuf,
    ssem,
    wsem,
    spsem,
    s0sem,
    ringw,
    rings,
    onesem,
    wysem,
):
    z = lax.axis_index("sp")
    y = lax.axis_index("fs")
    t = lax.axis_index("tp")
    x = t // 2
    c = t % 2
    y2 = y // 2
    y1 = y % 2
    other = 1 - c
    width = nz * NY * 32

    def dev(z_, y_, x_, c_):
        return {"sp": z_, "fs": y_, "tp": 2 * x_ + c_}

    partner = dev(z, y, x, other)
    up = dev((z + 1) % nz, y, x, c)
    down = dev((z + nz - 1) % nz, y, x, c)

    used = [0]
    pending = []

    def send(src, dst, rsem, to, local=None):
        sem = ssem.at[used[0]]
        used[0] += 1
        copy = pltpu.make_async_remote_copy(src, dst, sem, rsem, device_id=to, device_id_type=MESH)
        if local is None:
            copy.start()
            pending.append(copy.wait_send)
            return
        here = pltpu.make_async_copy(src, dst, rsem)
        away = jnp.logical_not(local)

        @pl.when(away)
        def _():
            copy.start()

        @pl.when(local)
        def _():
            here.start()

        def finish():
            @pl.when(away)
            def _():
                copy.wait_send()

        pending.append(finish)

    def drain(ref, sem):
        pltpu.make_async_copy(ref, ref, sem).wait()

    def ring(chunks, last_up, sems, arrived, hooks):
        half = nz // 2

        def carries(direction, i, k):
            return k < half or (i in last_up) == (direction == 0)

        def pass_on(k, i, direction, zi):
            if carries(direction, i, k + 1):
                ref = chunks[i](zi)
                send(ref, ref, sems.at[direction, k, i], up if direction == 0 else down)

        for i in range(len(chunks)):
            for direction in (0, 1):
                pass_on(0, i, direction, z)
            arrived(i, z)
        hooks(0)
        for k in range(1, half + 1):
            for i in range(len(chunks)):
                for direction in (0, 1):
                    if not carries(direction, i, k):
                        continue
                    zi = (z + nz - k) % nz if direction == 0 else (z + k) % nz
                    drain(chunks[i](zi), sems.at[direction, k - 1, i])
                    if k < half:
                        pass_on(k, i, direction, zi)
                    arrived(i, zi)
            hooks(k)

    STA, STB, XS, WD, WOD, WOWN, HALO, ACT, RS = range(9)

    own_out = pltpu.make_async_copy(wot, wob.at[c, z, y], onesem.at[WOWN])
    own_out.start()
    pltpu.make_async_copy(tok.at[pl.ds(0, 16)], sta.at[x], onesem.at[STA]).start()
    pltpu.make_async_copy(tok.at[pl.ds(16, 16)], stb.at[y], onesem.at[STB]).start()

    barrier = pltpu.get_barrier_semaphore()
    greeted = [partner, up, down]
    for d in range(1, NX):
        for core in (0, 1):
            greeted.append(dev(z, y, (x + d) % NX, core))
    for d in range(1, NY):
        for core in (0, 1):
            greeted.append(dev(z, (y + d) % NY, x, core))
    for peer in greeted:
        pl.semaphore_signal(barrier, inc=1, device_id=peer, device_id_type=MESH)
    pl.semaphore_wait(barrier, len(greeted))

    row = (z * NY + y) * 32
    for j in (0, 1):
        to = dev(z, 2 * c + j, x, y2)
        local = jnp.logical_and(y2 == c, y1 == j)
        pieces = [(wf, j * DK), (wv, j * DK), (wq, j * DK), (wg, 0), (wm, 0), (wi, 0)]
        for m, (ref, at) in enumerate(pieces):
            send(
                ref.at[:, pl.ds(at, DK)],
                wbuf.at[pl.ds(row, 32), pl.ds(m * DK, DK)],
                wsem.at[y1],
                to,
                local,
            )
    for d in range(1, NX):
        send(
            tok.at[pl.ds(0, 16)], sta.at[x], onesem.at[STA], dev(z, y, (x + d) % NX, c)
        )
        send(
            tok.at[pl.ds(16, 16)], stb.at[y], onesem.at[STB], dev(z, (y + d) % NY, x, c)
        )
    for j in (0, 1):
        to = dev(z, 2 * c + j, x, y2)
        local = jnp.logical_and(y2 == c, y1 == j)
        send(small.at[j], spbuf.at[y1], spsem.at[y1], to, local)
        send(s0.at[j], s0buf.at[y1], s0sem.at[y1], to, local)

    own_out.wait()
    for i in (0, 1):
        drain(wbuf.at[pl.ds(z * 128 + c * 64 + i * 32, 32)], wsem.at[i])

    def weight_chunk(i):
        return lambda zi: wbuf.at[pl.ds(pl.multiple_of(zi * 128 + c * 64 + i * 32, 32), 32)]

    def out_chunk(zi):
        return wob.at[c, zi, y]

    def weight_arrived(i, zi):
        if i < 2:
            ref = weight_chunk(i)(zi)
            send(ref, ref, onesem.at[WD], partner)

    def spread_tokens(k):
        if k != 1:
            return
        drain(sta, onesem.at[STA])
        for d in range(1, NY):
            send(sta, xbuf.at[y1, :, c, 0], onesem.at[XS], dev(z, (y + d) % NY, x, y2))
        send(sta, xbuf.at[y1, :, c, 0], onesem.at[XS], dev(z, y, x, y2), y2 == c)
        drain(stb, onesem.at[STB])
        for d in range(1, NX):
            for core in (0, 1):
                send(
                    stb.at[pl.ds(2 * core, 2)],
                    xbuf.at[:, x, c, 1],
                    onesem.at[XS],
                    dev(z, y, (x + d) % NX, core),
                )
        send(stb.at[pl.ds(2 * other, 2)], xbuf.at[:, x, c, 1], onesem.at[XS], partner)
        pltpu.make_async_copy(
            stb.at[pl.ds(2 * c, 2)], xbuf.at[:, x, c, 1], onesem.at[XS]
        ).start()

    ring([weight_chunk(0), weight_chunk(1), out_chunk], (0,), ringw, weight_arrived, spread_tokens)

    for d in range(1, NY):
        send(wob.at[c, :, y], wob.at[c, :, y], wysem.at[d - 1], dev(z, (y + d) % NY, x, c))
    send(wob.at[c, :, y], wob.at[c, :, y], onesem.at[WOD], partner)

    drain(xbuf, onesem.at[XS])
    drain(wbuf.at[pl.ds(0, width // 2)], onesem.at[WD])
    for i in (0, 1):
        drain(spbuf.at[i], spsem.at[i])

    rows = lax.broadcasted_iota(jnp.int32, (256, 256), 0)
    cols = lax.broadcasted_iota(jnp.int32, (256, 256), 1)
    causal = jnp.logical_and(rows // BLOCK == cols // BLOCK, cols <= rows)
    lower = jnp.where(causal, 1.0, 0.0).astype(BF16)
    word = lax.broadcasted_iota(jnp.int32, (16, DK), 0)

    def tokens_of(s):
        return xbuf[s].reshape(256, width)

    for s in (0, 1):
        fv = dot(tokens_of(s), wbuf[:, 0 : 2 * DK])
        forget = fv[:, :DK].astype(BF16).astype(F32)
        value = fv[:, DK:].astype(BF16)
        key_gate = spbuf[s, 0:1, :] * jax.nn.sigmoid(-forget)
        rates = jnp.concatenate(
            [
                jnp.transpose(jnp.broadcast_to(spbuf[s, 6 + h : 7 + h, :], (DK, DK)))
                for h in (0, 1)
            ],
            axis=0,
        )
        log_forget = jnp.log1p(-key_gate) + rates
        sums = dot(lower, jnp.concatenate(three_words(log_forget), axis=1))
        cum = sums[:, :DK] + sums[:, DK : 2 * DK] + sums[:, 2 * DK :]
        total = jnp.zeros((1, DK), F32)
        offsets = []
        for n in range(4):
            offsets.append(jnp.broadcast_to(total, (BLOCK, DK)))
            total = total + cum[n * BLOCK + BLOCK - 1 : n * BLOCK + BLOCK, :]
        offset = jnp.concatenate(offsets, axis=0)
        kept = (key_gate * jnp.exp(total - (cum + offset))).astype(BF16)
        sbuf[z, s, 0:DK, :] = dot_tn(value, kept).astype(BF16)
        high, middle, low = [
            jnp.broadcast_to(w.astype(F32), (16, DK)) for w in three_words(jnp.exp(total))
        ]
        words = jnp.where(word == 0, high, jnp.where(word == 1, middle, low))
        sbuf[z, s, DK : DK + 16, :] = words.astype(BF16)
        vbuf[s] = value
        kgbuf[s] = key_gate
        cumbuf[s] = cum
        offbuf[s] = offset

    def state_chunk(s):
        return lambda zi: sbuf.at[zi, s]

    def query_work():
        for s in (0, 1):
            q = dot(tokens_of(s), wbuf[:, 2 * DK : 3 * DK]).astype(BF16)
            qbuf[s] = q.astype(F32) * DK ** (-0.5)

    def conv_work():
        projected = dot(tokens_of(y1), wbuf[:, 3 * DK : 6 * DK]).astype(BF16).astype(F32)
        gatebuf[...] = projected[:, :DK]
        ext[8:264, :] = projected[:, DK : 2 * DK] * projected[:, 2 * DK :]
        send(ext.at[pl.ds(256, 8)], halo, onesem.at[HALO], up)

    def block_work(s):
        cum = cumbuf[s]
        key_gate = kgbuf[s]
        value = vbuf[s]
        decayed = qbuf[s] * jnp.exp(cum)
        qbbuf[s] = (decayed * jnp.exp(offbuf[s])).astype(BF16)
        queries = decayed.astype(BF16)
        keys = (key_gate * jnp.exp(-cum)).astype(BF16)
        scores = jnp.where(causal, dot_nt(queries, keys), 0.0).astype(BF16)
        recbuf[s] = dot(scores, value)
        entering = None
        for n in range(4):
            at = slice(n * BLOCK, n * BLOCK + BLOCK)
            final = cum[n * BLOCK + BLOCK - 1 : n * BLOCK + BLOCK, :]
            if entering is not None:
                recbuf[s, at, :] += dot_nt(queries[at], entering.astype(BF16))
            if n < 3:
                kept = (key_gate[at] * jnp.exp(final - cum[at])).astype(BF16)
                here = dot_tn(value[at], kept)
                entering = here if entering is None else jnp.exp(final) * entering + here

    def conv_finish():
        drain(halo, onesem.at[HALO])
        ext[0:8, :] = jnp.where(z == 0, 0.0, halo[...])
        conv = jnp.broadcast_to(spbuf[0, 5:6, :], (256, DK))
        for j in range(3):
            conv = conv + spbuf[0, 2 + j : 3 + j, :] * ext[6 + j : 262 + j, :]
        actc[...] = (gatebuf[...] * conv).astype(BF16).reshape(NX, 2, 32, DK)
        for core in (0, 1):
            send(
                actc.at[:, core],
                abuf.at[y2 * 3 + 2],
                onesem.at[ACT],
                dev(z, 2 * c + y1, x, core),
                jnp.logical_and(y2 == c, c == core),
            )

    def out_weights(d):
        ref = wob.at[c, :, (y + NY - d) % NY]
        drain(ref, wysem.at[d - 1])
        send(ref, ref, onesem.at[WOD], partner)

    def meanwhile(k):
        if k == 0:
            query_work()
        elif k == 1:
            conv_work()
        elif k == 2:
            block_work(0)
        elif k == 3:
            block_work(1)
        elif k == 4:
            conv_finish()

    ring([state_chunk(0), state_chunk(1)], (0,), rings, lambda i, zi: None, meanwhile)

    for d in range(1, NY):
        out_weights(d)

    for s in (0, 1):
        drain(s0buf.at[s], s0sem.at[s])
        carried = jnp.transpose(s0buf[s])
        for j in range(nz - 1):
            words = sbuf[j, s, DK : DK + 16, :].astype(F32)
            decay = words[0:1] + words[1:2] + words[2:3]
            later = decay * carried + sbuf[j, s, 0:DK, :].astype(F32)
            carried = jnp.where(j < z, later, carried)
        raw = recbuf[s] + dot_nt(qbbuf[s], carried.astype(BF16))
        mean_square = jnp.mean(raw * raw, axis=-1, keepdims=True)
        rec = raw * lax.rsqrt(mean_square + 1e-06) * spbuf[s, 1:2, :]
        actr[s] = rec.astype(BF16).reshape(NX, 2, 32, DK)
        for core in (0, 1):
            send(
                actr.at[s, :, core],
                abuf.at[y2 * 3 + y1],
                onesem.at[ACT],
                dev(z, 2 * c + s, x, core),
                jnp.logical_and(y == 2 * c + s, c == core),
            )

    drain(wob.at[other], onesem.at[WOD])
    drain(abuf, onesem.at[ACT])
    acts = [
        jnp.concatenate([abuf[3 * g + m].reshape(128, DK) for m in range(3)], axis=1)
        for g in (0, 1)
    ]
    for part in range(nz // 4):
        at = slice(4 * part, 4 * part + 4)
        partial = dot_nt(acts[0], wob[0, at].reshape(512, 3 * DK)) + dot_nt(
            acts[1], wob[1, at].reshape(512, 3 * DK)
        )
        pbuf[:, :, 512 * part : 512 * part + 512] = partial.astype(BF16).reshape(NX, 32, 512)
        for d in (2, 1, 3):
            to = (x + d) % NX
            cut = pl.ds(512 * part, 512)
            send(pbuf.at[to, :, cut], rbuf.at[x, :, cut], onesem.at[RS], dev(z, y, to, c))
    total = pbuf[x].astype(F32)
    drain(rbuf.at[pl.ds(0, NX - 1)], onesem.at[RS])
    for d in range(1, NX):
        total = total + rbuf[(x + d) % NX].astype(F32)
    out[...] = total.astype(BF16)
    for finish in pending:
        finish()


SENDS = 400


def shards(
    tokens,
    query_weight,
    forget_weight,
    value_weight,
    convolution_gate_weight,
    convolution_multiplier_weight,
    convolution_input_weight,
    gate_headroom,
    added_log_rate,
    initial_state,
    head_norm_gain,
    convolution_taps,
    convolution_bias,
    recurrence_output_weight,
    convolution_output_weight,
):
    nz = lax.axis_size("sp")
    width = tokens.shape[-1]

    def both(a):
        return jnp.broadcast_to(a[None], (2, *a.shape))

    small = jnp.concatenate(
        [
            gate_headroom.reshape(2, 1, DK),
            head_norm_gain.reshape(2, 1, DK),
            both(convolution_taps),
            both(convolution_bias.reshape(1, DK)),
            added_log_rate[0].reshape(2, 2, DK),
        ],
        axis=1,
    )
    out_weights = jnp.concatenate(
        [recurrence_output_weight.T, convolution_output_weight.T], axis=1
    )
    vmem = pl.BlockSpec(memory_space=pltpu.VMEM)
    call = pl.pallas_call(
        functools.partial(layer, nz),
        out_shape=jax.ShapeDtypeStruct((32, width), BF16),
        in_specs=[vmem] * 10,
        out_specs=vmem,
        scratch_shapes=[
            pltpu.VMEM((width, 6 * DK), BF16),
            pltpu.VMEM((2, nz, NY, 32, 3 * DK), BF16),
            pltpu.VMEM((2, NX, 2, 2, 16, width), BF16),
            pltpu.VMEM((NX, 16, width), BF16),
            pltpu.VMEM((NY, 16, width), BF16),
            pltpu.VMEM((2, 8, DK), F32),
            pltpu.VMEM((2, DK, DK), F32),
            pltpu.VMEM((nz, 2, DK + 16, DK), BF16),
            pltpu.VMEM((2, 256, DK), BF16),
            pltpu.VMEM((2, 256, DK), F32),
            pltpu.VMEM((2, 256, DK), F32),
            pltpu.VMEM((2, 256, DK), F32),
            pltpu.VMEM((2, 256, DK), F32),
            pltpu.VMEM((2, 256, DK), F32),
            pltpu.VMEM((2, 256, DK), BF16),
            pltpu.VMEM((256, DK), F32),
            pltpu.VMEM((264, DK), F32),
            pltpu.VMEM((8, DK), F32),
            pltpu.VMEM((2, NX, 2, 32, DK), BF16),
            pltpu.VMEM((NX, 2, 32, DK), BF16),
            pltpu.VMEM((6, NX, 32, DK), BF16),
            pltpu.VMEM((NX, 32, width), BF16),
            pltpu.VMEM((NX, 32, width), BF16),
            pltpu.SemaphoreType.DMA((SENDS,)),
            pltpu.SemaphoreType.DMA((2,)),
            pltpu.SemaphoreType.DMA((2,)),
            pltpu.SemaphoreType.DMA((2,)),
            pltpu.SemaphoreType.DMA((2, nz // 2, 3)),
            pltpu.SemaphoreType.DMA((2, nz // 2, 2)),
            pltpu.SemaphoreType.DMA((9,)),
            pltpu.SemaphoreType.DMA((NY - 1,)),
        ],
        compiler_params=pltpu.CompilerParams(collective_id=0, has_side_effects=True),
    )
    mixed = call(
        tokens[0],
        query_weight,
        forget_weight,
        value_weight,
        convolution_gate_weight,
        convolution_multiplier_weight,
        convolution_input_weight,
        small,
        initial_state[0],
        out_weights,
    )
    return mixed[None]


def solution(mesh):
    in_specs = (
        P("fs", ("sp", "tp"), None),
        P(("sp", "fs"), "tp"),
        P(("sp", "fs"), "tp"),
        P(("sp", "fs"), "tp"),
        P(("sp", "fs"), "tp"),
        P(("sp", "fs"), "tp"),
        P(("sp", "fs"), "tp"),
        P("tp"),
        P("fs", "tp", "sp"),
        P("fs", "tp", None, None),
        P("tp"),
        P(None, "tp"),
        P("tp"),
        P("tp", ("sp", "fs")),
        P("tp", ("sp", "fs")),
    )
    out_specs = P("fs", ("sp", "tp"), None)
    return jax.shard_map(shards, mesh=mesh, in_specs=in_specs, out_specs=out_specs, check_vma=False)
```

time: 288 us -> 101 us (0.35)
  the two profiles are of different devices: /device:TPU:496 before, /device:TPU:1 now
where the time goes in v1:
time: 101 us
  Pallas kernels  97.2 us (96%)
  local copies, waits for them, and re-layouts  2.98 us (3%)
    pallas_call x1, Pallas kernels, shards(): call(tokens[0], query_weight, forget_weight, value_weight, convolution_ga...  97.2 us
    unnamed x15, local copies, waits for them, and re-layouts  2.35 us

profile of v1, /device:TPU:1, one launch (start us, length us, event | category | flops | bytes accessed | tf_op | source)
XLA Modules:
  0.0 100.8 jit_solution(6417384029882555172)
XLA Ops:
  0.0 0.0 copy-start.6
  0.0 0.0 copy-start.3
  0.0 0.0 copy-start.2
  0.0 0.0 copy-start.4
  0.0 0.0 copy-start.5
  0.0 0.0 copy-start
  0.0 0.6 copy-done.6
  0.7 0.0 copy-done.3
  0.7 0.0 copy-done.2
  0.7 0.0 copy-done.4
  0.7 0.0 copy-done.5
  0.7 0.0 copy-start.1
  0.7 0.6 concatenate.6.small
  1.4 0.0 copy-done
  1.4 0.1 copy-done.1
  1.4 0.6 pad_maximum_fusion.wot
  2.1 97.2 %shard_map.145 = bf16[32,2048]{1,0:T(8,128)(2,1)} custom-call(bf16[32,2048]{1,0:T(8,128)(2,1)} %bitcast.8, bf16[32,256]{1,0:T(8,128)(2,1)} %wq.1, bf16[32,256]{1,0:T(8,128)(2,1)} %wf.1, bf16[32,256]{1,0:T(8,128)(2,1)} %wv.1, bf16[32,128]{1,0:T(8,128)(2,1)} %wg.1, bf16[32,128]{1,0:T(8,128)(2,1)} %wm.1, bf16[32,128]{1,0:T(8,128)(2,1)} %wi.1, ...), custom_call_target="tpu_custom_call" | custom-call | tf_op jit(solution)/shard_map/pallas_call | solution.py:494
  99.2 1.6 %copy.17 = bf16[1,32,2048]{2,1,0:T(8,128)(2,1)} copy(bf16[1,32,2048]{2,1,0:T(8,128)(2,1)} %bitcast.7) | data formatting | bytes 262144
  (3 shorter events, 0.0 us)
Async XLA Ops:
  0.0 0.7 copy-start.6
  0.0 0.7 copy-start.3
  0.0 0.7 copy-start.2
  0.0 0.7 copy-start.4
  0.0 0.7 copy-start.5
  0.0 1.3 %copy-start = (bf16[256,32]{0,1:T(8,128)(2,1)S(1)}, bf16[256,32]{0,1:T(8,128)(2,1)}, u32[]{:S(2)}) copy-start(bf16[256,32]{0,1:T(8,128)(2,1)} %param.28) | copy-start | bytes 49156
  0.7 0.7 copy-start.1
